TPU v7x, 32 devices: a whole 2x2x4 slice. The times are simulated.
32 devices in a mesh: ep: 8 (over z, x), tp: 4 (over y, core).
Axes of the slice: x: 2, y: 2, z: 4, core: 2. Of those that a mesh axis runs over, the one named last changes fastest.
Arguments:
- queries: bfloat16 [6144, 1024], P('ep', 'tp'), may hold values from -6.5 to 6.5
- keys: bfloat16 [6144, 1024], P('ep', 'tp'), may hold values from -6.5 to 6.5
- values: bfloat16 [6144, 1024], P('ep', 'tp'), may hold values from -6 to 6
- cum_gate: float32 [6144, 16], P('ep', 'tp'), may hold values from -770 to 0, as said below
- head_gain: float32 [1024], P('tp'), may hold values from 0.1 to 1.9
- moe_in: bfloat16 [1024, 2048], P('ep'), may hold values from -6 to 6
- ffn_gain: float32 [2048], replicated, may hold values from 0.1 to 1.9
- routes: int32 [1024, 4], P('ep'), may hold values from 0 to 31, all different within a row; in each aligned block of 128 rows (0 to 127, 128 to 255, ...) at most 24 rows name the same one
- route_weight: float32 [1024, 4], P('ep'), may hold values from 0.2 to 1.2
- expert_gate: bfloat16 [32, 1024, 2048], P('ep', 'tp'), may hold values from -0.125 to 0.125
- expert_up: bfloat16 [32, 1024, 2048], P('ep', 'tp'), may hold values from -0.125 to 0.125
- expert_down: bfloat16 [32, 1024, 2048], P('ep', 'tp'), may hold values from -0.25 to 0.25
- shared_gate: bfloat16 [512, 2048], P('tp'), may hold values from -0.125 to 0.125
- shared_up: bfloat16 [512, 2048], P('tp'), may hold values from -0.125 to 0.125
- shared_down: bfloat16 [512, 2048], P('tp'), may hold values from -0.375 to 0.375
Outputs:
- mixed: bfloat16 [6144, 1024], P('ep', 'tp')
- expert_out: bfloat16 [1024, 2048], P('ep', 'tp')
Inputs may be any that keep to these rules, and one draw needn't show every extreme that they name: `routes`: in each aligned block of 128 rows (the tokens of one index of ep) no expert is named by more than 24 rows, a bound that some block reaches; a row names 4 different experts. Each head's cum_gate never rises from one position to the next.
All inputs are finite; a program needn't handle non-finite values.
Results may differ from a plain program's by a relative error of at most 0.019.
Values may be sent and summed in bfloat16 or wider, within the bound.
A program may use at most 128 MiB of HBM per device.

v0:
```python
import functools
import math

import jax
import jax.numpy as jnp
from jax import lax
from jax.experimental import pallas as pl
from jax.experimental.pallas import tpu as pltpu
from jax.sharding import PartitionSpec as P

NORM_EPSILON = 1e-06
VMEM = pltpu.VMEM


def swap_halves(x):
    half = x.shape[1] // 2
    return jnp.concatenate([x[:, half:], x[:, :half]], axis=1)


def pack_kernel(splits, scale, q_ref, k_ref, v_ref, kv_ref, qp_ref):
    rows, width = q_ref.shape
    tile = rows // splits
    half = tile // 2
    low = lax.broadcasted_iota(jnp.int32, (rows, 128), 1) < 64
    low_half = low[:half]
    for head in range(width // 64):
        lanes = slice(head // 2 * 128, head // 2 * 128 + 128)
        kc, vc = k_ref[:, lanes], v_ref[:, lanes]
        qc = q_ref[:, lanes] * jnp.asarray(scale, q_ref.dtype)
        if head % 2 == 0:
            kv_ref[head] = jnp.where(low, kc, swap_halves(vc))
        else:
            kv_ref[head] = jnp.where(low, swap_halves(kc), vc)
        for part in range(splits):
            a = qc[part * tile : part * tile + half]
            b = qc[part * tile + half : (part + 1) * tile]
            if head % 2 == 0:
                packed = jnp.where(low_half, a, swap_halves(b))
            else:
                packed = jnp.where(low_half, swap_halves(a), b)
            qp_ref[head * splits + part] = packed


def flash_kernel(splits, packed, key_len, q_ref, kv_ref, gate_ref, gain_ref, out_ref):
    block = pl.program_id(0)
    part = lax.rem(lax.axis_index("ep"), splits)
    raw = q_ref[0]
    half = raw.shape[0]
    if packed:
        low = lax.broadcasted_iota(jnp.int32, raw.shape, 1) < 64
        zero = jnp.zeros_like(raw)
        query = jnp.concatenate(
            [jnp.where(low, raw, zero), jnp.where(low, swap_halves(raw), zero)], axis=0
        )
    else:
        query = raw
    rows = query.shape[0]

    def visit(step, state, masked):
        peak, weighted = state
        keys = kv_ref[pl.ds(pl.multiple_of(step * key_len, key_len), key_len), :]
        scores = lax.dot_general(
            query, keys, (((1,), (1,)), ((), ())), preferred_element_type=jnp.float32
        )
        scores = scores - gate_ref[step]
        if masked:
            row_pos = part * rows + lax.broadcasted_iota(jnp.int32, scores.shape, 0)
            key_pos = lax.broadcasted_iota(jnp.int32, scores.shape, 1)
            scores = jnp.where(key_pos <= row_pos, scores, -jnp.inf)
        new_peak = jnp.maximum(peak, jnp.max(scores, axis=1, keepdims=True))
        weights = jnp.exp(scores - new_peak).astype(jnp.bfloat16)
        weighted = weighted * jnp.exp(peak - new_peak) + jnp.dot(
            weights, keys, preferred_element_type=jnp.float32
        )
        return new_peak, weighted

    state = (jnp.full((rows, 1), -1e30, jnp.float32), jnp.zeros((rows, 128), jnp.float32))
    state = visit(block, state, True)
    state = lax.fori_loop(0, block, lambda step, s: visit(step, s, False), state)
    _, weighted = state
    high = lax.broadcasted_iota(jnp.int32, weighted.shape, 1) >= 64
    square = jnp.sum(jnp.where(high, weighted * weighted, 0.0), axis=1, keepdims=True) / 64
    normed = weighted * lax.rsqrt(square + NORM_EPSILON) * gain_ref[...]
    if packed:
        normed = jnp.where(high[:half], normed[half:], swap_halves(normed[:half]))
    out_ref[0] = normed.astype(out_ref.dtype)


def trade_small(cum_gate, routes, route_weight):
    rows, heads = cum_gate.shape
    devices = lax.axis_size("ep")
    tokens, choose = routes.shape
    gates = jnp.repeat(cum_gate.T, devices // heads, axis=0)
    named = jnp.concatenate([routes.astype(jnp.float32).reshape(-1), route_weight.reshape(-1)])
    small = jnp.concatenate([gates, jnp.broadcast_to(named, (devices, named.size))], axis=1)
    small = lax.all_to_all(small, "ep", split_axis=0, concat_axis=0, tiled=True)
    count = tokens * choose
    all_routes = small[:, rows : rows + count].astype(jnp.int32).reshape(-1, choose)
    all_weights = small[:, rows + count :].reshape(-1, choose)
    return small[:, :rows], all_routes, all_weights


def trade_rows(queries, keys, values, heads):
    rows, width = queries.shape
    size = width // heads
    devices = lax.axis_size("ep")
    splits = devices // heads
    tile = rows // splits
    scale = size**-0.5
    packed = heads % 2 == 0 and (tile // 2) % 16 == 0
    send_rows = tile // 2 if packed else tile
    if packed:
        kv, qp = pl.pallas_call(
            functools.partial(pack_kernel, splits, scale),
            out_shape=(
                jax.ShapeDtypeStruct((heads, rows, 128), jnp.bfloat16),
                jax.ShapeDtypeStruct((devices, send_rows, 128), jnp.bfloat16),
            ),
            name="pack",
        )(queries, keys, values)
    else:
        kv = jnp.concatenate(
            [keys.reshape(rows, heads, size), values.reshape(rows, heads, size)], axis=2
        ).transpose(1, 0, 2)
        qs = (queries * jnp.asarray(scale, queries.dtype)).reshape(splits, tile, heads, size)
        qs = qs.transpose(2, 0, 1, 3).reshape(devices, tile, size)
        qp = jnp.concatenate([qs, jnp.zeros_like(qs)], axis=2)
    parcel = jnp.concatenate([jnp.repeat(kv, splits, axis=0), qp], axis=1)
    return lax.all_to_all(parcel, "ep", split_axis=0, concat_axis=0, tiled=True), packed


def attend(got, packed, rows, all_gates, heads, head_gain):
    devices, parcel_rows, _ = got.shape
    width = head_gain.shape[0]
    size = width // heads
    splits = devices // heads
    tile = rows // splits
    send_rows = parcel_rows - rows
    kv_all = got[:, :rows].reshape(devices * rows, 128)
    q_all = got[:, rows:]
    head = lax.axis_index("ep") // splits
    gain = lax.dynamic_slice_in_dim(head_gain, head * size, size, 0)
    gain = jnp.concatenate([gain, gain])[None]
    flops = 2 * 2 * 128 * devices * (devices + 1) // 2 * tile * rows
    out = pl.pallas_call(
        functools.partial(flash_kernel, splits, packed, rows),
        grid=(devices,),
        in_specs=[
            pl.BlockSpec((1, send_rows, 128), lambda i: (i, 0, 0)),
            pl.BlockSpec(memory_space=VMEM),
            pl.BlockSpec(memory_space=VMEM),
            pl.BlockSpec(memory_space=VMEM),
        ],
        out_specs=pl.BlockSpec((1, send_rows, 128), lambda i: (i, 0, 0)),
        out_shape=jax.ShapeDtypeStruct((devices, send_rows, 128), jnp.bfloat16),
        cost_estimate=pl.CostEstimate(
            flops=flops, bytes_accessed=4 * devices * rows * 128, transcendentals=flops // 512
        ),
        compiler_params=pltpu.CompilerParams(vmem_limit_bytes=40 << 20),
        name="flash",
    )(q_all, kv_all, all_gates.reshape(devices, 1, rows), gain)
    back = lax.all_to_all(out, "ep", split_axis=0, concat_axis=0, tiled=True)
    if packed:
        back = back.reshape(heads, splits, tile // 2, 2, size).transpose(1, 3, 2, 0, 4)
    else:
        back = back[:, :, size:].reshape(heads, splits, tile, size).transpose(1, 2, 0, 3)
    return back.reshape(rows, width)


def norm_kernel(x_ref, gain_ref, out_ref):
    parts, _, width = x_ref.shape
    pieces = [x_ref[part].astype(jnp.float32) for part in range(parts)]
    square = sum(jnp.sum(p * p, axis=1, keepdims=True) for p in pieces) / (parts * width)
    factor = lax.rsqrt(square + NORM_EPSILON)
    for part, piece in enumerate(pieces):
        lanes = slice(part * width, (part + 1) * width)
        out_ref[:, lanes] = (piece * factor * gain_ref[:, lanes]).astype(out_ref.dtype)


def gated(rows, gate, up):
    dims = (((1,), (1,)), ((), ()))
    gate_value = lax.dot_general(rows, gate, dims, preferred_element_type=jnp.float32)
    up_value = lax.dot_general(rows, up, dims, preferred_element_type=jnp.float32)
    return gate_value / (1.0 + jnp.exp(-gate_value)) * up_value


def hidden_kernel(
    x_ref, routes_ref, weight_ref, gate_ref, up_ref, sgate_ref, sup_ref, hid_ref, shid_ref
):
    expert = pl.program_id(0)
    here = lax.axis_index("ep")
    tokens = shid_ref.shape[0]
    number = here * pl.num_programs(0) + expert
    chunk = min(256, x_ref.shape[0])

    @pl.loop(0, x_ref.shape[0] // chunk)
    def _(step):
        rows = pl.ds(pl.multiple_of(step * chunk, chunk), chunk)
        share = jnp.sum(
            jnp.where(routes_ref[rows, :] == number, weight_ref[rows, :], 0.0),
            axis=1,
            keepdims=True,
        )
        value = gated(x_ref[rows, :], gate_ref[0], up_ref[0])
        hid_ref[0, rows, :] = (value * share).astype(hid_ref.dtype)

    @pl.when(expert == 0)
    def _():
        own = x_ref[pl.ds(pl.multiple_of(here * tokens, tokens), tokens), :]
        shid_ref[...] = gated(own, sgate_ref[...], sup_ref[...]).astype(shid_ref.dtype)


def down_kernel(hid_ref, shid_ref, down_ref, sdown_ref, out_ref):
    tokens = shid_ref.shape[0]
    here = lax.axis_index("ep")
    per_group = down_ref.shape[0]

    @pl.loop(0, hid_ref.shape[1] // tokens)
    def _(step):
        rows = pl.ds(pl.multiple_of(step * tokens, tokens), tokens)
        term = sum(
            jnp.dot(hid_ref[expert, rows, :], down_ref[expert], preferred_element_type=jnp.float32)
            for expert in range(per_group)
        )
        out_ref[0, rows, :] = term.astype(out_ref.dtype)

        @pl.when(step == here)
        def _():
            extra = jnp.dot(shid_ref[...], sdown_ref[...], preferred_element_type=jnp.float32)
            out_ref[0, rows, :] = (term + extra).astype(out_ref.dtype)


def gather_tokens(moe_in):
    slice_width = moe_in.shape[1] // lax.axis_size("tp")
    own_columns = lax.dynamic_slice_in_dim(
        moe_in, lax.axis_index("tp") * slice_width, slice_width, 1
    )
    return lax.all_gather(own_columns, ("ep", "tp"), axis=0)


def expert_terms(
    gathered,
    ffn_gain,
    all_routes,
    all_weights,
    expert_gate,
    expert_up,
    expert_down,
    shared_gate,
    shared_up,
    shared_down,
):
    tokens = gathered.shape[1]
    model_width = ffn_gain.shape[0]
    per_group, hidden_width = expert_gate.shape[:2]
    shared_width = shared_gate.shape[0]
    groups = lax.axis_size("ep")
    parts = lax.axis_size("tp")
    slice_width = model_width // parts
    total = groups * tokens
    params = pltpu.CompilerParams(vmem_limit_bytes=48 << 20)
    whole = pl.BlockSpec(memory_space=VMEM)
    normed = pl.pallas_call(
        norm_kernel,
        grid=(groups,),
        in_specs=[pl.BlockSpec((parts, tokens, slice_width), lambda i: (i, 0, 0)), whole],
        out_specs=pl.BlockSpec((tokens, model_width), lambda i: (i, 0)),
        out_shape=jax.ShapeDtypeStruct((total, model_width), jnp.bfloat16),
        cost_estimate=pl.CostEstimate(
            flops=4 * total * model_width, bytes_accessed=4 * total * model_width, transcendentals=0
        ),
        name="norm",
    )(gathered, ffn_gain[None])
    weight_spec = pl.BlockSpec((1, hidden_width, model_width), lambda i: (i, 0, 0))
    columns = per_group * hidden_width
    hidden, shared_hidden = pl.pallas_call(
        hidden_kernel,
        grid=(per_group,),
        in_specs=[whole, whole, whole, weight_spec, weight_spec, whole, whole],
        out_specs=(
            pl.BlockSpec((1, total, hidden_width), lambda i: (i, 0, 0)),
            pl.BlockSpec((tokens, shared_width), lambda i: (0, 0)),
        ),
        out_shape=(
            jax.ShapeDtypeStruct((per_group, total, hidden_width), jnp.bfloat16),
            jax.ShapeDtypeStruct((tokens, shared_width), jnp.bfloat16),
        ),
        cost_estimate=pl.CostEstimate(
            flops=4 * total * model_width * columns,
            bytes_accessed=4 * columns * model_width,
            transcendentals=total * columns,
        ),
        compiler_params=params,
        name="hidden",
    )(normed, all_routes, all_weights, expert_gate, expert_up, shared_gate, shared_up)
    return pl.pallas_call(
        down_kernel,
        grid=(parts,),
        in_specs=[
            whole,
            whole,
            pl.BlockSpec((per_group, hidden_width, slice_width), lambda i: (0, 0, i)),
            pl.BlockSpec((shared_width, slice_width), lambda i: (0, i)),
        ],
        out_specs=pl.BlockSpec((1, total, slice_width), lambda i: (i, 0, 0)),
        out_shape=jax.ShapeDtypeStruct((parts, total, slice_width), jnp.bfloat16),
        cost_estimate=pl.CostEstimate(
            flops=2 * total * model_width * columns,
            bytes_accessed=2 * (columns + total) * model_width,
            transcendentals=0,
        ),
        compiler_params=params,
        name="down",
    )(hidden, shared_hidden, expert_down, shared_down)


def combine_terms(term):
    groups = lax.axis_size("ep")
    _, total, slice_width = term.shape
    tokens = total // groups
    summed = lax.psum_scatter(term, "tp", scatter_dimension=0, tiled=True)
    back = lax.all_to_all(
        summed.reshape(groups, tokens, slice_width), "ep", split_axis=0, concat_axis=0, tiled=True
    )
    return jnp.sum(back.astype(jnp.float32), axis=0).astype(jnp.bfloat16)


def on_device(
    queries,
    keys,
    values,
    cum_gate,
    head_gain,
    moe_in,
    ffn_gain,
    routes,
    route_weight,
    expert_gate,
    expert_up,
    expert_down,
    shared_gate,
    shared_up,
    shared_down,
):
    rows, heads = cum_gate.shape
    gathered = gather_tokens(moe_in)
    got, packed = trade_rows(queries, keys, values, heads)
    all_gates, all_routes, all_weights = trade_small(cum_gate, routes, route_weight)
    gathered, got = lax.optimization_barrier((gathered, got))
    term = expert_terms(
        gathered,
        ffn_gain,
        all_routes,
        all_weights,
        expert_gate,
        expert_up,
        expert_down,
        shared_gate,
        shared_up,
        shared_down,
    )
    term, got = lax.optimization_barrier((term, got))
    mixed = attend(got, packed, rows, all_gates, heads, head_gain)
    return (mixed, combine_terms(term))


def solution(mesh):
    in_specs = (
        P("ep", "tp"),
        P("ep", "tp"),
        P("ep", "tp"),
        P("ep", "tp"),
        P("tp"),
        P("ep", None),
        P(),
        P("ep", None),
        P("ep", None),
        P("ep", "tp", None),
        P("ep", "tp", None),
        P("ep", "tp", None),
        P("tp", None),
        P("tp", None),
        P("tp", None),
    )
    out_specs = (P("ep", "tp"), P("ep", "tp"))
    return jax.shard_map(
        on_device, mesh=mesh, in_specs=in_specs, out_specs=out_specs, check_vma=False
    )
```

profile of v0, /device:TPU:0, one launch (start us, length us, event | category | flops | bytes accessed | tf_op | source)
XLA Modules:
  0.0 218.2 jit_solution(5721029527298938819)
XLA Ops:
  7.2 1.0 copy-done
  8.2 0.7 constant_dynamic-slice_fusion
  8.9 0.7 convert_element_type.8
  9.6 0.1 copy.23
  9.7 0.1 reshape.41
  9.8 0.8 copy.24
  10.7 0.7 broadcast_in_dim.17
  11.5 0.7 all_to_all.18
  12.1 7.3 %all-to-all-start.1 = ((f32[8,1,1792]{2,1,0:T(1,128)}), f32[8,1,1792]{2,1,0:T(1,128)S(1)}, u32[]{:S(2)}, u32[]{:S(2)}) async-start(f32[8,1,1792]{2,1,0:T(1,128)} %all_to_all.18), calls=%async_computation.1 | async-start | bytes 114688 | tf_op jit(solution)/shard_map/all_to_all | solution.py:96
  19.4 2.6 %pack.1 = (bf16[4,768,128]{2,1,0:T(8,128)(2,1)}, bf16[8,192,128]{2,1,0:T(8,128)(2,1)}) custom-call(bf16[768,256]{1,0:T(8,128)(2,1)} %q_ref.1, bf16[768,256]{1,0:T(8,128)(2,1)} %k_ref.1, bf16[768,256]{1,0:T(8,128)(2,1)} %v_ref.1), custom_call_target="tpu_custom_call" | custom-call | tf_op jit(solution)/shard_map/pack/pallas_call | solution.py:113
  22.0 1.4 broadcast_in_dim.15
  23.4 2.4 %pad_maximum_fusion = bf16[8,960,128]{2,1,0:T(8,128)(2,1)} fusion(bf16[8,192,128]{2,1,0:T(8,128)(2,1)} %get-tuple-element.11, bf16[8,768,128]{2,1,0:T(8,128)(2,1)S(1)} %bitcast.15), kind=kLoop, calls=%fused_computation | loop fusion | flops 3932160 | bytes 3932160 | tf_op jit(solution)/shard_map/concatenate | solution.py:128
  25.8 0.6 all-to-all-done.1
  26.4 5.4 %all-to-all-start = ((bf16[8,960,128]{2,1,0:T(8,128)(2,1)}), bf16[8,960,128]{2,1,0:T(8,128)(2,1)S(1)}, u32[]{:S(2)}, u32[]{:S(2)}) async-start(bf16[8,960,128]{2,1,0:T(8,128)(2,1)} %pad_maximum_fusion), calls=%async_computation | async-start | bytes 3932160 | tf_op jit(solution)/shard_map/all_to_all | solution.py:129
  31.9 0.6 copy-done.6
  32.5 0.5 reshape.43.routes_ref
  33.0 0.5 reshape.44.weight_ref
  33.6 49.0 %all-to-all-done = bf16[8,960,128]{2,1,0:T(8,128)(2,1)S(1)} async-done(((bf16[8,960,128]{2,1,0:T(8,128)(2,1)}), bf16[8,960,128]{2,1,0:T(8,128)(2,1)S(1)}, u32[]{:S(2)}, u32[]{:S(2)}) %all-to-all-start) | async-done | bytes 1966112 | tf_op jit(solution)/shard_map/all_to_all | solution.py:129
  82.6 15.4 %all-gather.3.cloned.1.call-done = bf16[4096,512]{1,0:T(8,128)(2,1)} async-done(((bf16[128,512]{1,0:T(8,128)(2,1)}), bf16[4096,512]{1,0:T(8,128)(2,1)}) %all-gather.3.cloned.1.call-update) | async-done | bytes 4194320 | tf_op jit(solution)/shard_map/all_gather | solution.py:238
  98.0 7.6 %norm.1.x_ref = bf16[1024,2048]{1,0:T(8,128)(2,1)} custom-call(bf16[32,128,512]{2,1,0:T(8,128)(2,1)} %bitcast.16, f32[1,2048]{1,0:T(1,128)} %bitcast.22), custom_call_target="tpu_custom_call" | custom-call | flops 8388608 | bytes 8388608 | tf_op jit(solution)/shard_map/norm/pallas_call | solution.py:263
  105.6 15.7 %hidden.1 = (bf16[4,1024,256]{2,1,0:T(8,128)(2,1)S(1)}, bf16[128,128]{1,0:T(8,128)(2,1)S(1)}) custom-call(bf16[1024,2048]{1,0:T(8,128)(2,1)} %norm.1.x_ref, s32[1024,4]{1,0:T(8,128)S(1)} %reshape.43.routes_ref, f32[1024,4]{1,0:T(8,128)S(1)} %reshape.44.weight_ref, bf16[4,256,2048]{2,1,0:T(8,128)(2,1)} %gate_ref.1, bf16[4,256,2048]{2,1,0:T(8,128)(2,1)} %up_ref.1, ...), custom_call_target="tpu_custom_call" | custom-call | flops 8589934592 | bytes 8388608 | tf_op jit(solution)/shard_map/hidden/pallas_call | solution.py:276
  121.4 13.0 %down.1 = bf16[4,1024,512]{2,1,0:T(8,128)(2,1)} custom-call(bf16[4,1024,256]{2,1,0:T(8,128)(2,1)S(1)} %get-tuple-element.13.hid_ref, bf16[128,128]{1,0:T(8,128)(2,1)S(1)} %get-tuple-element.14.shid_ref, bf16[4,256,2048]{2,1,0:T(8,128)(2,1)} %down_ref.1, bf16[128,2048]{1,0:T(8,128)(2,1)S(1)} %copy-done.3), custom_call_target="tpu_custom_call" | custom-call | flops 4294967296 | bytes 8388608 | tf_op jit(solution)/shard_map/down/pallas_call | solution.py:296
  134.4 0.6 copy-done.7
  135.2 0.7 slice.22
  136.1 29.0 %flash.1 = bf16[8,192,128]{2,1,0:T(8,128)(2,1)S(1)} custom-call(bf16[8,192,128]{2,1,0:T(8,128)(2,1)S(1)} %slice.17.q_ref, bf16[6144,128]{1,0:T(8,128)(2,1)S(1)} %bitcast.14, f32[8,1,768]{2,1,0:T(1,128)S(1)} %reshape.46.gate_ref, f32[1,128]{1,0:T(1,128)S(1)} %maximum_bitcast_fusion.gain_ref), custom_call_target="tpu_custom_call" | custom-call | flops 5435817984 | bytes 3145728 | tf_op jit(solution)/shard_map/flash/pallas_call | solution.py:145
  165.1 16.4 %all_to_all.27 = bf16[8,192,128]{2,1,0:T(8,128)(2,1)S(1)} all-to-all(bf16[8,192,128]{2,1,0:T(8,128)(2,1)S(1)} %flash.1), channel_id=1, replica_groups=mesh['ep'=8,'tp'=4] {'ep'}, dimensions={0} | all-to-all | bytes 786432 | tf_op jit(solution)/shard_map/all_to_all | solution.py:162
  181.5 3.6 %all-to-all-start.3 = ((bf16[8,128,512]{2,1,0:T(8,128)(2,1)}), bf16[8,128,512]{2,1,0:T(8,128)(2,1)S(1)}, u32[]{:S(2)}, u32[]{:S(2)}) async-start(bf16[8,128,512]{2,1,0:T(8,128)(2,1)} %bitcast.18), calls=%async_computation.4 | async-start | bytes 2097152 | tf_op jit(solution)/shard_map/all_to_all | solution.py:322
  185.0 0.2 copy.25
  185.3 0.6 copy.28
  185.8 1.2 reshape.51
  187.1 23.4 %all-to-all-done.3 = bf16[8,128,512]{2,1,0:T(8,128)(2,1)S(1)} async-done(((bf16[8,128,512]{2,1,0:T(8,128)(2,1)}), bf16[8,128,512]{2,1,0:T(8,128)(2,1)S(1)}, u32[]{:S(2)}, u32[]{:S(2)}) %all-to-all-start.3) | async-done | bytes 1048608 | tf_op jit(solution)/shard_map/all_to_all | solution.py:322
  210.5 0.8 reduce_sum.12
  (29 shorter events, 0.6 us)
Async XLA Ops:
  7.2 1.0 copy-start
  7.2 90.8 %all-gather.3.cloned.1.call-start = ((), (), s32[]{:S(2)}) async-start(), calls=%async_computation.6 | async-start | bytes 4325376 | tf_op jit(solution)/shard_map/all_gather | solution.py:238
  12.1 14.2 %all-to-all-start.1 = ((f32[8,1,1792]{2,1,0:T(1,128)}), f32[8,1,1792]{2,1,0:T(1,128)S(1)}, u32[]{:S(2)}, u32[]{:S(2)}) async-start(f32[8,1,1792]{2,1,0:T(1,128)} %all_to_all.18), calls=%async_computation.1 | async-start | bytes 114688 | tf_op jit(solution)/shard_map/all_to_all | solution.py:96
  26.4 56.2 %all-to-all-start = ((bf16[8,960,128]{2,1,0:T(8,128)(2,1)}), bf16[8,960,128]{2,1,0:T(8,128)(2,1)S(1)}, u32[]{:S(2)}, u32[]{:S(2)}) async-start(bf16[8,960,128]{2,1,0:T(8,128)(2,1)} %pad_maximum_fusion), calls=%async_computation | async-start | bytes 3932160 | tf_op jit(solution)/shard_map/all_to_all | solution.py:129
  31.8 149.7 %reduce-scatter.2.cloned.1.call-start = ((), (), s32[]{:S(2)}) async-start(), calls=%async_computation.5 | async-start | bytes 5242880 | tf_op jit(solution)/shard_map/reduce_scatter | solution.py:321
  31.9 0.6 copy-start.6
  82.6 15.4 %copy-start.4 = (bf16[8,960,128]{2,1,0:T(8,128)(2,1)}, bf16[8,960,128]{2,1,0:T(8,128)(2,1)S(1)}, u32[]{:S(2)}) copy-start(bf16[8,960,128]{2,1,0:T(8,128)(2,1)S(1)} %all-to-all-done) | copy-start | bytes 5898244
  98.0 7.6 %copy-start.1 = (bf16[128,2048]{1,0:T(8,128)(2,1)S(1)}, bf16[128,2048]{1,0:T(8,128)(2,1)}, u32[]{:S(2)}) copy-start(bf16[128,2048]{1,0:T(8,128)(2,1)} %sgate_ref.1) | copy-start | bytes 1572868
  98.0 7.6 %copy-start.2 = (bf16[128,2048]{1,0:T(8,128)(2,1)S(1)}, bf16[128,2048]{1,0:T(8,128)(2,1)}, u32[]{:S(2)}) copy-start(bf16[128,2048]{1,0:T(8,128)(2,1)} %sup_ref.1) | copy-start | bytes 1572868
  105.6 15.8 %copy-start.3 = (bf16[128,2048]{1,0:T(8,128)(2,1)S(1)}, bf16[128,2048]{1,0:T(8,128)(2,1)}, u32[]{:S(2)}) copy-start(bf16[128,2048]{1,0:T(8,128)(2,1)} %sdown_ref.1) | copy-start | bytes 1572868
  134.4 0.7 copy-start.7
  134.4 1.6 copy-start.5
  181.5 29.0 %all-to-all-start.3 = ((bf16[8,128,512]{2,1,0:T(8,128)(2,1)}), bf16[8,128,512]{2,1,0:T(8,128)(2,1)S(1)}, u32[]{:S(2)}, u32[]{:S(2)}) async-start(bf16[8,128,512]{2,1,0:T(8,128)(2,1)} %bitcast.18), calls=%async_computation.4 | async-start | bytes 2097152 | tf_op jit(solution)/shard_map/all_to_all | solution.py:322
Sparse Core Ops, SparseCore 0:
  11.4 86.5 all-gather.2
  134.5 43.3 reduce-scatter.1
where the time goes:
time: 219 us; the launch traced here: 218 us
  waiting for transfers between devices  88.4 us (40%)
  Pallas kernels  67.9 us (31%)
  starting transfers between devices  16.4 us (7%)
  blocking collectives  16.4 us (7%)
  between operations  14.2 us (6%)
  local copies, waits for them, and re-layouts  10.9 us (5%)
  other arithmetic  4.02 us (2%)
    all_to_all x1, waiting for transfers between devices, trade_rows(): lax.all_to_all(parcel, 'ep', split_axis=0, concat_axis=0, tiled=True)  49 us
    pallas_call x1, Pallas kernels, attend(): pl.pallas_call(functools.partial(flash_kernel, splits, packed, rows), gri...  29 us
    all_to_all x1, waiting for transfers between devices, combine_terms(): lax.all_to_all(summed.reshape(groups, tokens, slice_width), 'ep', split_a...  23.4 us
    all_to_all x1, blocking collectives, attend(): back = lax.all_to_all(out, 'ep', split_axis=0, concat_axis=0, tiled=True)  16.4 us
    pallas_call x1, Pallas kernels, expert_terms(): pl.pallas_call(hidden_kernel, grid=(per_group,), in_specs=[whole, whole,...  15.7 us
    all_gather x1, waiting for transfers between devices, gather_tokens(): return lax.all_gather(own_columns, ('ep', 'tp'), axis=0)  15.4 us
    pallas_call x1, Pallas kernels, expert_terms(): pl.pallas_call(down_kernel, grid=(parts,), in_specs=[whole, whole, pl.Blo...  13 us
    pallas_call x1, Pallas kernels, expert_terms(): pl.pallas_call(norm_kernel, grid=(groups,), in_specs=[pl.BlockSpec((parts...  7.6 us
  transfers between devices with their start and end apart: 5, of which 4 were waited for; matrix products, arithmetic and copies ran while one was open for 5% of the time, Pallas kernels for 14%

commit v1 on v0

--- a/solution.py
+++ b/solution.py
@@ -325,6 +325,657 @@
     return jnp.sum(back.astype(jnp.float32), axis=0).astype(jnp.bfloat16)
 
 
+MESH = pl.DeviceIdType.MESH
+COPIES = 64
+
+
+def flipped(number, mask, bits=3):
+    total = 0
+    for bit in range(bits):
+        digit = lax.rem(number // (1 << bit), 2)
+        total = total + ((1 - digit) if (mask >> bit) & 1 else digit) * (1 << bit)
+    return total
+
+
+def fused_kernel(
+    cap,
+    q_ref,
+    k_ref,
+    v_ref,
+    small_ref,
+    gain_ref,
+    moe_ref,
+    ffn_ref,
+    egate_hbm,
+    eup_hbm,
+    edown_hbm,
+    sgate_hbm,
+    sup_hbm,
+    sdown_hbm,
+    mixed_ref,
+    expert_ref,
+    kvs,
+    qs,
+    kv_all,
+    q_all,
+    small_all,
+    peak_buf,
+    acc_buf,
+    o_send,
+    o_recv,
+    x_all,
+    xg,
+    sel_buf,
+    share_buf,
+    egate,
+    eup,
+    edown,
+    sgate,
+    sup,
+    sdown,
+    y_buf,
+    ysh,
+    r1,
+    r1s,
+    s_send,
+    ss_send,
+    r2,
+    r2s,
+    term_buf,
+    t_send,
+    r3,
+    u_send,
+    r4,
+    wsem,
+    send_sem,
+    recv_sem,
+):
+    e = lax.axis_index("ep")
+    t = lax.axis_index("tp")
+    z, x = e // 2, lax.rem(e, 2)
+    y, c = t // 2, lax.rem(t, 2)
+    ty = (1 - y) * 2 + c
+    tc = y * 2 + 1 - c
+    rows, width = q_ref.shape
+    heads = width // 64
+    tile = rows // 2
+    half = tile // 2
+    tokens, model = moe_ref.shape
+    quarter = model // 4
+    per_group, hid, _ = egate.shape
+    slot2 = 2 * cap
+    slots = per_group * slot2
+
+    def peer(m):
+        return flipped(e, m)
+
+    def pair(k):
+        return flipped(z, k, 2)
+
+    ids = {}
+
+    def remote(name, src, dst, device):
+        n = ids.setdefault(name, len(ids))
+        return pltpu.make_async_remote_copy(
+            src_ref=src,
+            dst_ref=dst,
+            send_sem=send_sem.at[n],
+            recv_sem=recv_sem.at[n],
+            device_id=device,
+            device_id_type=MESH,
+        )
+
+    def block(b, col, count=1):
+        return x_all.at[
+            pl.ds(pl.multiple_of(b * tokens, tokens), count * tokens),
+            pl.ds(pl.multiple_of(col * quarter, quarter), quarter),
+        ]
+
+    def small(m):
+        return remote(
+            ("small", m), small_ref.at[pair(m // 2)], small_all.at[e], {"ep": peer(m)}
+        )
+
+    def gz(k):
+        return remote(("gz", k), block(e, t), block(e, t), {"ep": peer(2 * k)})
+
+    def gx(k):
+        b = peer(2 * k)
+        return remote(("gx", k), block(b, t), block(b, t), {"ep": peer(1)})
+
+    def pair_rows(k, col):
+        if k == 0:
+            return block(peer(1), col)
+        return block(pair(k) * 2, col, 2)
+
+    def gy(k):
+        return remote(("gy", k), pair_rows(k, t), pair_rows(k, t), {"tp": ty})
+
+    def gd0(k):
+        return remote(("gd0", k), pair_rows(k, t), pair_rows(k, t), {"tp": tc})
+
+    def gd1(k):
+        return remote(("gd1", k), pair_rows(k, ty), pair_rows(k, ty), {"tp": tc})
+
+    def kvz(k):
+        return remote(("kvz", k), kvs.at[pair(k)], kv_all.at[e], {"ep": peer(2 * k)})
+
+    def kvx(k):
+        b = peer(2 * k)
+        return remote(("kvx", k), kv_all.at[b], kv_all.at[b], {"ep": peer(1)})
+
+    def qc(m):
+        part = (1 - x) if m % 2 else x
+        return remote(("q", m), qs.at[pair(m // 2), part], q_all.at[e], {"ep": peer(m)})
+
+    def c_r1(k):
+        return remote(("r1", k), y_buf.at[1 - c, :, k], r1.at[:, k], {"tp": tc})
+
+    def c_r1s():
+        return remote("r1s", ysh.at[1 - c], r1s, {"tp": tc})
+
+    def c_r2(k):
+        return remote(("r2", k), s_send.at[k], r2.at[k], {"tp": ty})
+
+    def c_r2s():
+        return remote("r2s", ss_send, r2s, {"tp": ty})
+
+    def c_r3(k):
+        return remote(("r3", k), t_send.at[k], r3.at[k], {"ep": peer(1)})
+
+    def c_r4(k):
+        return remote(("r4", k), u_send.at[k], r4.at[k], {"ep": peer(2 * k)})
+
+    def c_o(m):
+        return remote(("o", m), o_send.at[peer(m)], o_recv.at[e], {"ep": peer(m)})
+
+    started = []
+
+    def start(copy_fn, *args):
+        copy_fn(*args).start()
+        started.append((copy_fn, args))
+
+    barrier = pltpu.get_barrier_semaphore()
+    for m in range(1, 8):
+        pl.semaphore_signal(barrier, inc=1, device_id={"ep": peer(m)}, device_id_type=MESH)
+    for other in (ty, tc):
+        pl.semaphore_signal(barrier, inc=1, device_id={"tp": other}, device_id_type=MESH)
+
+    loads = [
+        pltpu.make_async_copy(src, dst, wsem.at[n])
+        for n, (src, dst) in enumerate(
+            (
+                (sgate_hbm, sgate),
+                (sup_hbm, sup),
+                (sdown_hbm, sdown),
+                (egate_hbm, egate),
+                (eup_hbm, eup),
+                (edown_hbm, edown),
+            )
+        )
+    ]
+    for load in loads:
+        load.start()
+
+    own = moe_ref[...].astype(jnp.float32)
+    square = jnp.sum(own * own, axis=1, keepdims=True) / model
+    own = (own * lax.rsqrt(square + NORM_EPSILON) * ffn_ref[...]).astype(jnp.bfloat16)
+    own_rows = pl.ds(pl.multiple_of(e * tokens, tokens), tokens)
+    x_all[own_rows, :] = own
+    small_all[e] = small_ref[z]
+
+    pl.semaphore_wait(barrier, 9)
+    for k in (1, 2, 3):
+        start(gz, k)
+    start(gx, 0)
+    for m in range(1, 8):
+        start(small, m)
+
+    low = lax.broadcasted_iota(jnp.int32, (rows, 128), 1) < 64
+    low_half = low[:half]
+    for head in range(heads):
+        lanes = slice(head // 2 * 128, head // 2 * 128 + 128)
+        kc, vc = k_ref[:, lanes], v_ref[:, lanes]
+        qq = q_ref[:, lanes] * jnp.asarray(0.125, q_ref.dtype)
+        if head % 2 == 0:
+            kvs[head] = jnp.where(low, kc, swap_halves(vc))
+        else:
+            kvs[head] = jnp.where(low, swap_halves(kc), vc)
+        for part in range(2):
+            a = qq[part * tile : part * tile + half]
+            b = qq[part * tile + half : (part + 1) * tile]
+            if head % 2 == 0:
+                packed = jnp.where(low_half, a, swap_halves(b))
+            else:
+                packed = jnp.where(low_half, swap_halves(a), b)
+            qs[head, part] = packed
+    kv_all[e] = kvs[z]
+    q_all[e] = qs[z, x]
+    start(kvx, 0)
+    start(qc, 1)
+    for k in (1, 2, 3):
+        start(kvz, k)
+        start(qc, 2 * k)
+        start(qc, 2 * k + 1)
+
+    peak_buf[...] = jnp.full(peak_buf.shape, -1e30, jnp.float32)
+    acc_buf[...] = jnp.zeros(acc_buf.shape, jnp.float32)
+
+    low_q = low_half
+    high = lax.broadcasted_iota(jnp.int32, (tile, 128), 1) >= 64
+
+    def visit(i, j, masked):
+        raw = q_all[i]
+        zero = jnp.zeros_like(raw)
+        query = jnp.concatenate(
+            [jnp.where(low_q, raw, zero), jnp.where(low_q, swap_halves(raw), zero)], axis=0
+        )
+        keys = kv_all[j]
+        scores = lax.dot_general(
+            query, keys, (((1,), (1,)), ((), ())), preferred_element_type=jnp.float32
+        )
+        gates = jnp.concatenate(
+            [small_all[j, 8 + r : 9 + r, :] for r in range(rows // 128)], axis=1
+        )
+        scores = scores - gates
+        if masked:
+            row_pos = x * tile + lax.broadcasted_iota(jnp.int32, scores.shape, 0)
+            key_pos = lax.broadcasted_iota(jnp.int32, scores.shape, 1)
+            scores = jnp.where(key_pos <= row_pos, scores, -jnp.inf)
+        peak = peak_buf[i]
+        new_peak = jnp.maximum(peak, jnp.max(scores, axis=1, keepdims=True))
+        weights = jnp.exp(scores - new_peak).astype(jnp.bfloat16)
+        acc_buf[i] = acc_buf[i] * jnp.exp(peak - new_peak) + jnp.dot(
+            weights, keys, preferred_element_type=jnp.float32
+        )
+        peak_buf[i] = new_peak
+
+    def diagonal(k):
+        pk = pair(k)
+
+        @pl.loop(0, 2)
+        def _(v):
+            visit(2 * pk + v, 2 * pk + v, True)
+
+    def visits(k, first, last, events=None):
+        pk = pair(k)
+
+        @pl.loop(first, last)
+        def _(v):
+            inner = (v + 63) // 64
+            u = v + 1 - inner - inner
+            m = u // 4 + (1 - inner) * 0
+            pm = 0
+            for bit in range(2):
+                digit = lax.rem(lax.rem(z // (1 << bit), 2) + lax.rem(m // (1 << bit), 2), 2)
+                pm = pm + digit * (1 << bit)
+            above = (pk - pm + 4) // 4
+            hi = pm + above * (pk - pm)
+            lo = pk - above * (pk - pm)
+            i = inner * (2 * hi + lax.rem(u // 2, 2)) + (1 - inner) * (2 * pk + 1)
+            j = inner * (2 * lo + lax.rem(u, 2)) + (1 - inner) * (2 * pk)
+            visit(i, j, False)
+            for at, event in (events or {}).items():
+                pl.when(v == at)(event)
+
+    def epilogue(k):
+        for xx in range(2):
+            m = 2 * k + xx
+            i = peer(m)
+            weighted = acc_buf[i]
+            square = jnp.sum(jnp.where(high, weighted * weighted, 0.0), axis=1, keepdims=True) / 64
+            out = weighted * lax.rsqrt(square + NORM_EPSILON) * gain_ref[z]
+            out = jnp.where(high[:half], out[half:], swap_halves(out[:half]))
+            out = out.astype(o_send.dtype)
+            if m == 0:
+                o_recv[e] = out
+            else:
+                o_send[i] = out
+                start(c_o, m)
+
+    upper = (
+        lax.broadcasted_iota(jnp.int32, (tokens, tokens), 0)
+        <= lax.broadcasted_iota(jnp.int32, (tokens, tokens), 1)
+    )
+    upper = jnp.where(upper, 1.0, 0.0).astype(jnp.bfloat16)
+
+    def select(k):
+        pk = pair(k)
+        named, chosen = [], []
+        for bb in range(2):
+            table = small_all[2 * pk + bb]
+            ids_of = table[0:4].astype(jnp.int32)
+            share = table[4:8]
+            for j in range(per_group):
+                hit = ids_of == e * per_group + j
+                named.append(jnp.sum(jnp.where(hit, 1.0, 0.0), axis=0, keepdims=True))
+                chosen.append(jnp.sum(jnp.where(hit, share, 0.0), axis=0, keepdims=True))
+        flags = jnp.concatenate(named, axis=0)
+        rank = jnp.dot(flags.astype(jnp.bfloat16), upper, preferred_element_type=jnp.float32)
+        slot = jnp.where(flags > 0.5, rank - 1.0, -1000.0)
+        row_of = lax.broadcasted_iota(jnp.int32, (slot2, 2 * tokens), 0).astype(jnp.float32)
+        for j in range(per_group):
+            target = jnp.concatenate(
+                [slot[j : j + 1], slot[per_group + j : per_group + j + 1] + float(cap)], axis=1
+            )
+            share = jnp.concatenate([chosen[j], chosen[per_group + j]], axis=1)
+            match = row_of == target
+            sel_buf[k, j * slot2 : (j + 1) * slot2, :] = jnp.where(match, 1.0, 0.0).astype(
+                jnp.bfloat16
+            )
+            share_buf[j, k * slot2 : (k + 1) * slot2, :] = jnp.sum(
+                jnp.where(match, share, 0.0), axis=1, keepdims=True
+            )
+
+    def pick(k):
+        gd0(k).wait_recv()
+        gd1(k).wait_recv()
+        pair_at = pl.ds(pl.multiple_of(pair(k) * 2 * tokens, 2 * tokens), 2 * tokens)
+        for part in range(4):
+            cols = slice(part * quarter, (part + 1) * quarter)
+            picked = jnp.dot(
+                sel_buf[k], x_all[pair_at, cols], preferred_element_type=jnp.float32
+            ).astype(jnp.bfloat16)
+            for j in range(per_group):
+                xg[j, k * slot2 : (k + 1) * slot2, cols] = picked[j * slot2 : (j + 1) * slot2]
+
+    def e1(k):
+        gz(k).wait_recv()
+        start(gx, k)
+
+    def e2(k):
+        gx(k).wait_recv()
+        start(gy, k)
+        start(gd0, k)
+
+    def e3(k):
+        gy(k).wait_recv()
+        start(gd1, k)
+
+    def forward(k):
+        kvz(k).wait_recv()
+        start(kvx, k)
+
+    def ready(k):
+        kvx(k).wait_recv()
+        for m in (2 * k, 2 * k + 1):
+            if m:
+                qc(m).wait_recv()
+
+    for load in loads[:3]:
+        load.wait()
+    shared_hidden = gated(x_all[own_rows, :], sgate[...], sup[...]).astype(jnp.bfloat16)
+    for part in range(4):
+        cols = slice(part * quarter, (part + 1) * quarter)
+        ysh[part % 2, part // 2] = jnp.dot(
+            shared_hidden, sdown[:, cols], preferred_element_type=jnp.float32
+        ).astype(jnp.bfloat16)
+    e2(0)
+    e1(1)
+    e2(1)
+    for m in range(1, 8):
+        small(m).wait_recv()
+    for k in range(4):
+        select(k)
+    e1(2)
+    e3(0)
+    e2(2)
+    e1(3)
+    e2(3)
+    ready(0)
+    diagonal(0)
+    visits(0, 0, 1)
+    e3(1)
+    pick(0)
+    forward(1)
+    pick(1)
+    e3(2)
+    ready(1)
+    diagonal(1)
+    visits(1, 0, 5)
+    e3(3)
+    pick(2)
+    forward(2)
+    pick(3)
+    for load in loads[3:]:
+        load.wait()
+
+    @pl.loop(0, per_group)
+    def _(j):
+        value = gated(xg[j], egate[j], eup[j])
+        hidden = (value * share_buf[j]).astype(jnp.bfloat16)
+        at = pl.ds(pl.multiple_of(j * slot2, 16), slot2)
+        for part in range(4):
+            cols = slice(part * quarter, (part + 1) * quarter)
+            out = jnp.dot(
+                hidden, edown[j, :, cols], preferred_element_type=jnp.float32
+            ).astype(jnp.bfloat16)
+            for k in range(4):
+                y_buf[part % 2, part // 2, k, at, :] = out[k * slot2 : (k + 1) * slot2]
+
+    for k in (3, 2, 1, 0):
+        start(c_r1, k)
+    start(c_r1s)
+
+    def wide(ref):
+        return ref.astype(jnp.float32)
+
+    def core_sum(k):
+        c_r1(k).wait_recv()
+        s_send[k] = (wide(y_buf[c, 1 - y, k]) + wide(r1[1 - y, k])).astype(jnp.bfloat16)
+        c_r2(k).start()
+
+    def shared_sum():
+        c_r1s().wait_recv()
+        ss_send[...] = (wide(ysh[c, 1 - y]) + wide(r1s[1 - y])).astype(jnp.bfloat16)
+        c_r2s().start()
+
+    def scatter(k):
+        c_r2(k).wait_recv()
+        total = wide(y_buf[c, y, k]) + wide(r1[y, k]) + wide(r2[k])
+        term = lax.dot_general(
+            sel_buf[k],
+            total.astype(jnp.bfloat16),
+            (((0,), (0,)), ((), ())),
+            preferred_element_type=jnp.float32,
+        )
+        term_buf[k, 0] = term[:tokens]
+        term_buf[k, 1] = term[tokens:]
+        t_send[k] = term_buf[k, 1 - x].astype(jnp.bfloat16)
+        c_r3(k).start()
+
+    def combine(k):
+        c_r3(k).wait_recv()
+        u_send[k] = (term_buf[k, x] + wide(r3[k])).astype(jnp.bfloat16)
+        c_r4(k).start()
+
+    for k in range(4):
+        started.append((c_r2, (k,)))
+        started.append((c_r3, (k,)))
+        if k:
+            started.append((c_r4, (k,)))
+    started.append((c_r2s, ()))
+
+    forward(3)
+    core_sum(3)
+    core_sum(2)
+    ready(2)
+    diagonal(2)
+    core_sum(1)
+    core_sum(0)
+    shared_sum()
+    visits(2, 0, 9)
+    scatter(3)
+    ready(3)
+    diagonal(3)
+    visits(3, 0, 5)
+    epilogue(0)
+    combine(3)
+    scatter(2)
+    visits(3, 5, 9)
+    epilogue(1)
+    combine(2)
+    scatter(1)
+    visits(3, 9, 13)
+    epilogue(2)
+    epilogue(3)
+    combine(1)
+    scatter(0)
+    c_r2s().wait_recv()
+    c_r3(0).wait_recv()
+    out = term_buf[0, x] + wide(r3[0]) + wide(ysh[c, y]) + wide(r1s[y]) + wide(r2s[...])
+    for k in (3, 2, 1):
+        c_r4(k).wait_recv()
+        out = out + wide(r4[k])
+    expert_ref[...] = out.astype(expert_ref.dtype)
+
+    for m in range(1, 8):
+        c_o(m).wait_recv()
+    for part in range(2):
+        for head in range(0, heads, 2):
+            lanes = slice(head // 2 * 128, head // 2 * 128 + 128)
+            first, second = o_recv[head * 2 + part], o_recv[(head + 1) * 2 + part]
+            at = part * tile
+            mixed_ref[at : at + half, lanes] = jnp.where(low_half, first, swap_halves(second))
+            mixed_ref[at + half : at + tile, lanes] = jnp.where(
+                low_half, swap_halves(first), second
+            )
+    for copy_fn, args in started:
+        copy_fn(*args).wait_send()
+
+
+def fused(
+    queries,
+    keys,
+    values,
+    cum_gate,
+    head_gain,
+    moe_in,
+    ffn_gain,
+    routes,
+    route_weight,
+    expert_gate,
+    expert_up,
+    expert_down,
+    shared_gate,
+    shared_up,
+    shared_down,
+):
+    rows, heads = cum_gate.shape
+    width = queries.shape[1]
+    tokens, model = moe_in.shape
+    choose = routes.shape[1]
+    per_group, hid, _ = expert_gate.shape
+    experts = per_group * lax.axis_size("ep")
+    cap = 3 * tokens * choose // (2 * experts)
+    devices = lax.axis_size("ep")
+    tile, half, quarter = rows // 2, rows // 4, model // 4
+    slots = per_group * 2 * cap
+    shared = shared_gate.shape[0]
+    lines = rows // 128
+    gates = cum_gate.T.reshape(heads, lines, 128)
+    named = jnp.concatenate([routes.astype(jnp.float32), route_weight], axis=1).T
+    small = jnp.concatenate(
+        [
+            jnp.broadcast_to(named, (heads, 2 * choose, 128)),
+            gates,
+            jnp.zeros((heads, 8 - lines, 128), jnp.float32),
+        ],
+        axis=1,
+    )
+    gain = head_gain.reshape(heads, 1, 64)
+    gain = jnp.concatenate([gain, gain], axis=2)
+    bf16, f32 = jnp.bfloat16, jnp.float32
+    vmem = pl.BlockSpec(memory_space=VMEM)
+    hbm = pl.BlockSpec(memory_space=pl.ANY)
+    scratch = [
+        VMEM((heads, rows, 128), bf16),
+        VMEM((heads, 2, half, 128), bf16),
+        VMEM((devices, rows, 128), bf16),
+        VMEM((devices, half, 128), bf16),
+        VMEM((devices, 16, 128), f32),
+        VMEM((devices, tile, 1), f32),
+        VMEM((devices, tile, 128), f32),
+        VMEM((devices, half, 128), bf16),
+        VMEM((devices, half, 128), bf16),
+        VMEM((devices * tokens, model), bf16),
+        VMEM((per_group, 8 * cap, model), bf16),
+        VMEM((4, slots, 2 * tokens), bf16),
+        VMEM((per_group, 8 * cap, 1), f32),
+        VMEM((per_group, hid, model), bf16),
+        VMEM((per_group, hid, model), bf16),
+        VMEM((per_group, hid, model), bf16),
+        VMEM((shared, model), bf16),
+        VMEM((shared, model), bf16),
+        VMEM((shared, model), bf16),
+        VMEM((2, 2, 4, slots, quarter), bf16),
+        VMEM((2, 2, tokens, quarter), bf16),
+        VMEM((2, 4, slots, quarter), bf16),
+        VMEM((2, tokens, quarter), bf16),
+        VMEM((4, slots, quarter), bf16),
+        VMEM((tokens, quarter), bf16),
+        VMEM((4, slots, quarter), bf16),
+        VMEM((tokens, quarter), bf16),
+        VMEM((4, 2, tokens, quarter), f32),
+        VMEM((4, tokens, quarter), bf16),
+        VMEM((4, tokens, quarter), bf16),
+        VMEM((4, tokens, quarter), bf16),
+        VMEM((4, tokens, quarter), bf16),
+        pltpu.SemaphoreType.DMA((6,)),
+        pltpu.SemaphoreType.DMA((COPIES,)),
+        pltpu.SemaphoreType.DMA((COPIES,)),
+    ]
+    return pl.pallas_call(
+        functools.partial(fused_kernel, cap),
+        in_specs=[vmem] * 7 + [hbm] * 6,
+        out_specs=(vmem, vmem),
+        out_shape=(
+            jax.ShapeDtypeStruct((rows, width), bf16),
+            jax.ShapeDtypeStruct((tokens, quarter), bf16),
+        ),
+        scratch_shapes=scratch,
+        compiler_params=pltpu.CompilerParams(
+            collective_id=0, has_side_effects=True, vmem_limit_bytes=62 << 20
+        ),
+        name="fused",
+    )(
+        queries,
+        keys,
+        values,
+        small,
+        gain,
+        moe_in,
+        ffn_gain[None],
+        expert_gate,
+        expert_up,
+        expert_down,
+        shared_gate,
+        shared_up,
+        shared_down,
+    )
+
+
+def fits_fused(cum_gate, queries, moe_in, routes, expert_gate):
+    rows, heads = cum_gate.shape
+    tokens, choose = routes.shape
+    per_group = expert_gate.shape[0]
+    devices = lax.axis_size("ep")
+    cap = 3 * tokens * choose // (2 * per_group * devices)
+    return (
+        devices == 8
+        and lax.axis_size("tp") == 4
+        and heads == 4
+        and queries.shape[1] == 256
+        and rows % 128 == 0
+        and rows // 128 <= 8
+        and (rows // 4) % 16 == 0
+        and tokens == 128
+        and choose == 4
+        and per_group == 4
+        and (2 * cap) % 16 == 0
+    )
+
+
 def on_device(
     queries,
     keys,
@@ -342,6 +993,24 @@
     shared_up,
     shared_down,
 ):
+    if fits_fused(cum_gate, queries, moe_in, routes, expert_gate):
+        return fused(
+            queries,
+            keys,
+            values,
+            cum_gate,
+            head_gain,
+            moe_in,
+            ffn_gain,
+            routes,
+            route_weight,
+            expert_gate,
+            expert_up,
+            expert_down,
+            shared_gate,
+            shared_up,
+            shared_down,
+        )
     rows, heads = cum_gate.shape
     gathered = gather_tokens(moe_in)
     got, packed = trade_rows(queries, keys, values, heads)

time: 219 us -> 106 us (0.48)
  waiting for transfers between devices: 88.4 us -> 0 us
  Pallas kernels: 67.9 us -> 97.3 us
  blocking collectives: 16.4 us -> 0 us
  starting transfers between devices: 16.4 us -> 0 us
  between operations: 14.2 us -> 0.65 us
  local copies, waits for them, and re-layouts: 10.9 us -> 4.89 us
    all_to_all x3 -> x0, waiting for transfers between devices: 73 us -> none  [the longest x1 49 us: trade_rows(): lax.all_to_all(parcel, 'ep', split_axis=0, concat_axis=0, tiled=True)]
    pallas_call x5 -> x1, Pallas kernels: 67.9 us -> 97.3 us  [fused(): pl.pallas_call(functools.partial(fused_kernel, cap), in_specs=[vmem] * 7...]
    all_to_all x1 -> x0, blocking collectives: 16.4 us -> none  [attend(): back = lax.all_to_all(out, 'ep', split_axis=0, concat_axis=0, tiled=True)]
    all_to_all x3 -> x0, starting transfers between devices: 16.3 us -> none  [the longest x1 7.28 us: trade_small(): small = lax.all_to_all(small, 'ep', split_axis=0, concat_axis=0, tiled=True)]
    all_gather x1 -> x0, waiting for transfers between devices: 15.4 us -> none  [gather_tokens(): return lax.all_gather(own_columns, ('ep', 'tp'), axis=0)]
    unnamed x20 -> x2, local copies, waits for them, and re-layouts: 4.85 us -> 3.33 us
  transfers between devices with their start and end apart: 5 -> 0, of which waited for: 4 -> 0; matrix products, arithmetic and copies ran while one was open for 5% -> 0% of each run, Pallas kernels for 14% -> 0%
where the time goes in v1:
time: 106 us
  Pallas kernels  97.3 us (92%)
  local copies, waits for them, and re-layouts  4.89 us (5%)
  other arithmetic  2.71 us (3%)
    pallas_call x1, Pallas kernels, fused(): pl.pallas_call(functools.partial(fused_kernel, cap), in_specs=[vmem] * 7...  97.3 us
    unnamed x2, local copies, waits for them, and re-layouts  3.33 us

profile of v1, /device:TPU:0, one launch (start us, length us, event | category | flops | bytes accessed | tf_op | source)
XLA Modules:
  0.0 105.5 jit_solution(15380621296678423351)
XLA Ops:
  0.6 0.1 pad.4.clone
  0.7 0.8 reshape.11
  1.5 0.7 pad_maximum_fusion.gain_ref
  2.1 0.7 convert_element_type.3
  2.8 0.7 maximum_bitcast_fusion
  3.5 0.7 reshape.10
  4.2 0.7 maximum_maximum_fusion.small_ref
  4.9 97.3 %fused.1 = (bf16[768,256]{1,0:T(8,128)(2,1)}, bf16[128,512]{1,0:T(8,128)(2,1)}) custom-call(bf16[768,256]{1,0:T(8,128)(2,1)} %q_ref.1, bf16[768,256]{1,0:T(8,128)(2,1)} %k_ref.1, bf16[768,256]{1,0:T(8,128)(2,1)} %v_ref.1, f32[4,16,128]{2,1,0:T(8,128)} %maximum_maximum_fusion.small_ref, f32[4,1,128]{2,1,0:T(1,128)} %pad_maximum_fusion.gain_ref, ...), custom_call_target="tpu_custom_call" | custom-call | tf_op jit(solution)/shard_map/fused/pallas_call | solution.py:928
  102.2 1.8 %copy.19 = bf16[768,256]{1,0:T(8,128)(2,1)} copy(bf16[768,256]{1,0:T(8,128)(2,1)} %get-tuple-element.4) | data formatting | bytes 786432
  104.0 1.6 %copy.20 = bf16[128,512]{1,0:T(8,128)(2,1)} copy(bf16[128,512]{1,0:T(8,128)(2,1)} %get-tuple-element.5) | data formatting | bytes 262144
  (2 shorter events, 0.0 us)

commit v2 on v1

--- a/solution.py
+++ b/solution.py
@@ -327,6 +327,7 @@
 
 MESH = pl.DeviceIdType.MESH
 COPIES = 64
+LOG2E = math.log2(math.e)
 
 
 def flipped(number, mask, bits=3):
@@ -342,7 +343,9 @@
     q_ref,
     k_ref,
     v_ref,
-    small_ref,
+    cum_ref,
+    routes_ref,
+    weight_ref,
     gain_ref,
     moe_ref,
     ffn_ref,
@@ -354,10 +357,14 @@
     sdown_hbm,
     mixed_ref,
     expert_ref,
+    small_ref,
     kvs,
     qs,
     kv_all,
     q_all,
+    kg,
+    vt,
+    qx,
     small_all,
     peak_buf,
     acc_buf,
@@ -437,7 +444,8 @@
         )
 
     def gz(k):
-        return remote(("gz", k), block(e, t), block(e, t), {"ep": peer(2 * k)})
+        b, to = (peer(4), peer(2)) if k == 3 else (e, peer(2 * k))
+        return remote(("gz", k), block(b, t), block(b, t), {"ep": to})
 
     def gx(k):
         b = peer(2 * k)
@@ -484,7 +492,8 @@
         return remote(("r3", k), t_send.at[k], r3.at[k], {"ep": peer(1)})
 
     def c_r4(k):
-        return remote(("r4", k), u_send.at[k], r4.at[k], {"ep": peer(2 * k)})
+        to = peer(2) if k == 3 else peer(2 * k)
+        return remote(("r4", k), u_send.at[k], r4.at[k], {"ep": to})
 
     def c_o(m):
         return remote(("o", m), o_send.at[peer(m)], o_recv.at[e], {"ep": peer(m)})
@@ -522,21 +531,24 @@
     own = (own * lax.rsqrt(square + NORM_EPSILON) * ffn_ref[...]).astype(jnp.bfloat16)
     own_rows = pl.ds(pl.multiple_of(e * tokens, tokens), tokens)
     x_all[own_rows, :] = own
+
+    lines = rows // 128
+    for head in range(heads):
+        small_ref[head, 0:4, :] = routes_ref[...].astype(jnp.float32)
+        small_ref[head, 4:8, :] = weight_ref[...]
+        small_ref[head, 8:16, :] = jnp.concatenate(
+            [cum_ref[head : head + 1, r * 128 : (r + 1) * 128] for r in range(lines)]
+            + [jnp.zeros((8 - lines, 128), jnp.float32)],
+            axis=0,
+        )
     small_all[e] = small_ref[z]
-
-    pl.semaphore_wait(barrier, 9)
-    for k in (1, 2, 3):
-        start(gz, k)
-    start(gx, 0)
-    for m in range(1, 8):
-        start(small, m)
 
     low = lax.broadcasted_iota(jnp.int32, (rows, 128), 1) < 64
     low_half = low[:half]
     for head in range(heads):
         lanes = slice(head // 2 * 128, head // 2 * 128 + 128)
         kc, vc = k_ref[:, lanes], v_ref[:, lanes]
-        qq = q_ref[:, lanes] * jnp.asarray(0.125, q_ref.dtype)
+        qq = q_ref[:, lanes]
         if head % 2 == 0:
             kvs[head] = jnp.where(low, kc, swap_halves(vc))
         else:
@@ -551,86 +563,125 @@
             qs[head, part] = packed
     kv_all[e] = kvs[z]
     q_all[e] = qs[z, x]
-    start(kvx, 0)
-    start(qc, 1)
-    for k in (1, 2, 3):
-        start(kvz, k)
-        start(qc, 2 * k)
-        start(qc, 2 * k + 1)
-
-    peak_buf[...] = jnp.full(peak_buf.shape, -1e30, jnp.float32)
-    acc_buf[...] = jnp.zeros(acc_buf.shape, jnp.float32)
-
-    low_q = low_half
-    high = lax.broadcasted_iota(jnp.int32, (tile, 128), 1) >= 64
-
-    def visit(i, j, masked):
-        raw = q_all[i]
-        zero = jnp.zeros_like(raw)
-        query = jnp.concatenate(
-            [jnp.where(low_q, raw, zero), jnp.where(low_q, swap_halves(raw), zero)], axis=0
-        )
-        keys = kv_all[j]
-        scores = lax.dot_general(
-            query, keys, (((1,), (1,)), ((), ())), preferred_element_type=jnp.float32
-        )
-        gates = jnp.concatenate(
-            [small_all[j, 8 + r : 9 + r, :] for r in range(rows // 128)], axis=1
-        )
-        scores = scores - gates
-        if masked:
-            row_pos = x * tile + lax.broadcasted_iota(jnp.int32, scores.shape, 0)
-            key_pos = lax.broadcasted_iota(jnp.int32, scores.shape, 1)
-            scores = jnp.where(key_pos <= row_pos, scores, -jnp.inf)
-        peak = peak_buf[i]
-        new_peak = jnp.maximum(peak, jnp.max(scores, axis=1, keepdims=True))
-        weights = jnp.exp(scores - new_peak).astype(jnp.bfloat16)
-        acc_buf[i] = acc_buf[i] * jnp.exp(peak - new_peak) + jnp.dot(
-            weights, keys, preferred_element_type=jnp.float32
-        )
-        peak_buf[i] = new_peak
+    pl.semaphore_wait(barrier, 9)
+    for m in (7, 6, 5, 4, 3, 2, 1):
+        start(small, m)
+    start(gz, 1)
+    start(gz, 2)
+    start(gx, 0)
+
+    lane = lax.broadcasted_iota(jnp.int32, (1, 128), 1)
+    spread = jnp.where(
+        lax.broadcasted_iota(jnp.int32, (16, 128), 0) + 64
+        == lax.broadcasted_iota(jnp.int32, (16, 128), 1),
+        1.0,
+        0.0,
+    )
+    gate_lane = lax.broadcasted_iota(jnp.int32, (16, 128), 0) < 3
+    spread = jnp.where(gate_lane, spread, 0.0).astype(jnp.bfloat16)
+    pick_value = jnp.where(
+        lax.broadcasted_iota(jnp.int32, (64, 128), 0) + 64
+        == lax.broadcasted_iota(jnp.int32, (64, 128), 1),
+        1.0,
+        0.0,
+    ).astype(jnp.bfloat16)
+    unit = jnp.where(lane < 67, 1.0, 0.0).astype(jnp.bfloat16)
+    both = (((1,), (1,)), ((), ()))
+
+    def prep_kv(j):
+        kv = kv_all[j]
+        left = small_all[j, 8:16, :] * -LOG2E
+        split = []
+        for _ in range(3):
+            piece = left.astype(jnp.bfloat16).astype(jnp.float32)
+            split.append(jnp.concatenate([piece[r : r + 1] for r in range(lines)], axis=1))
+            left = left - piece
+        split.append(jnp.zeros((13, rows), jnp.float32))
+        split = jnp.concatenate(split, axis=0).astype(jnp.bfloat16)
+        gates = lax.dot_general(
+            split, spread, (((0,), (0,)), ((), ())), preferred_element_type=jnp.float32
+        )
+        kg[j] = jnp.where(low, kv, gates.astype(jnp.bfloat16))
+        vt[j] = lax.dot_general(
+            pick_value, kv, both, preferred_element_type=jnp.float32
+        ).astype(jnp.bfloat16)
+
+    def prep_q(i):
+        raw = q_all[i].astype(jnp.float32) * (LOG2E * 64**-0.5)
+        first = raw.astype(jnp.bfloat16)
+        second = (raw - first.astype(jnp.float32)).astype(jnp.bfloat16)
+        zero = jnp.zeros_like(first)
+        for n, (value, rest) in enumerate(((first, zero), (second, zero + unit))):
+            qx[i, :, n * 128 : (n + 1) * 128] = jnp.concatenate(
+                [jnp.where(low_half, value, rest), jnp.where(low_half, swap_halves(value), rest)],
+                axis=0,
+            )
+
+    def scores_of(j, query):
+        keys = jnp.concatenate([kv_all[j], kg[j]], axis=1)
+        return lax.dot_general(keys, query, both, preferred_element_type=jnp.float32)
+
+    def update(j, scores, peak, out):
+        new_peak = jnp.maximum(peak, jnp.max(scores, axis=0, keepdims=True))
+        weights = jnp.exp2(scores - new_peak).astype(jnp.bfloat16)
+        out = out * jnp.exp2(peak - new_peak) + jnp.dot(
+            vt[j], weights, preferred_element_type=jnp.float32
+        )
+        return new_peak, out
 
     def diagonal(k):
         pk = pair(k)
-
-        @pl.loop(0, 2)
-        def _(v):
-            visit(2 * pk + v, 2 * pk + v, True)
-
-    def visits(k, first, last, events=None):
-        pk = pair(k)
-
-        @pl.loop(first, last)
-        def _(v):
-            inner = (v + 63) // 64
-            u = v + 1 - inner - inner
-            m = u // 4 + (1 - inner) * 0
-            pm = 0
-            for bit in range(2):
-                digit = lax.rem(lax.rem(z // (1 << bit), 2) + lax.rem(m // (1 << bit), 2), 2)
-                pm = pm + digit * (1 << bit)
-            above = (pk - pm + 4) // 4
-            hi = pm + above * (pk - pm)
-            lo = pk - above * (pk - pm)
-            i = inner * (2 * hi + lax.rem(u // 2, 2)) + (1 - inner) * (2 * pk + 1)
-            j = inner * (2 * lo + lax.rem(u, 2)) + (1 - inner) * (2 * pk)
-            visit(i, j, False)
-            for at, event in (events or {}).items():
-                pl.when(v == at)(event)
+        first, second = qx[2 * pk], qx[2 * pk + 1]
+        query = jnp.concatenate([first, second], axis=0)
+        scores = scores_of(2 * pk, query)
+        later = scores_of(2 * pk + 1, second)
+        key_pos = lax.broadcasted_iota(jnp.int32, (rows, 2 * tile), 0)
+        row_pos = lax.broadcasted_iota(jnp.int32, (rows, 2 * tile), 1)
+        allowed = (key_pos <= row_pos + x * tile) | (row_pos >= tile)
+        scores = jnp.where(allowed, scores, -jnp.inf)
+        peak = jnp.max(scores, axis=0, keepdims=True)
+        weights = jnp.exp2(scores - peak).astype(jnp.bfloat16)
+        out = jnp.dot(vt[2 * pk], weights, preferred_element_type=jnp.float32)
+        key_pos = lax.broadcasted_iota(jnp.int32, (rows, tile), 0)
+        row_pos = lax.broadcasted_iota(jnp.int32, (rows, tile), 1)
+        later = jnp.where(key_pos <= row_pos + x * tile, later, -jnp.inf)
+        last_peak, last_out = update(2 * pk + 1, later, peak[:, tile:], out[:, tile:])
+        peak_buf[pk, :, :tile] = peak[:, :tile]
+        peak_buf[pk, :, tile:] = last_peak
+        acc_buf[pk, :, :tile] = out[:, :tile]
+        acc_buf[pk, :, tile:] = last_out
+
+    def cross(k, m):
+        pk, pm = pair(k), pair(m)
+        above = (pk - pm + 4) // 4
+        hi = pm + above * (pk - pm)
+        lo = pk - above * (pk - pm)
+        query = jnp.concatenate([qx[2 * hi], qx[2 * hi + 1]], axis=0)
+        scores = scores_of(2 * lo, query)
+        later = scores_of(2 * lo + 1, query)
+        peak, out = update(2 * lo, scores, peak_buf[hi], acc_buf[hi])
+        peak, out = update(2 * lo + 1, later, peak, out)
+        peak_buf[hi] = peak
+        acc_buf[hi] = out
+
+    gain_pair = jnp.where(z // 2 == 0, gain_ref[:, :128], gain_ref[:, 128:])
+    gain_swap = swap_halves(gain_pair)
+    gain = jnp.where((lane < 64) == (lax.rem(z, 2) == 0), gain_pair, gain_swap)
 
     def epilogue(k):
+        weighted = acc_buf[pair(k)]
+        square = jnp.sum(weighted * weighted, axis=0, keepdims=True) / 64
+        normed = weighted * lax.rsqrt(square + NORM_EPSILON)
         for xx in range(2):
-            m = 2 * k + xx
-            i = peer(m)
-            weighted = acc_buf[i]
-            square = jnp.sum(jnp.where(high, weighted * weighted, 0.0), axis=1, keepdims=True) / 64
-            out = weighted * lax.rsqrt(square + NORM_EPSILON) * gain_ref[z]
-            out = jnp.where(high[:half], out[half:], swap_halves(out[:half]))
-            out = out.astype(o_send.dtype)
+            at = xx * tile
+            out = jnp.concatenate(
+                [normed[:, at : at + half], normed[:, at + half : at + tile]], axis=0
+            ).T
+            o_send[2 * pair(k) + xx] = (out * gain).astype(o_send.dtype)
+        for m in (2 * k, 2 * k + 1):
             if m == 0:
-                o_recv[e] = out
+                o_recv[e] = o_send[e]
             else:
-                o_send[i] = out
                 start(c_o, m)
 
     upper = (
@@ -701,6 +752,8 @@
         for m in (2 * k, 2 * k + 1):
             if m:
                 qc(m).wait_recv()
+            prep_kv(peer(m))
+            prep_q(peer(m))
 
     for load in loads[:3]:
         load.wait()
@@ -710,52 +763,24 @@
         ysh[part % 2, part // 2] = jnp.dot(
             shared_hidden, sdown[:, cols], preferred_element_type=jnp.float32
         ).astype(jnp.bfloat16)
-    e2(0)
-    e1(1)
-    e2(1)
-    for m in range(1, 8):
-        small(m).wait_recv()
-    for k in range(4):
-        select(k)
-    e1(2)
-    e3(0)
-    e2(2)
-    e1(3)
-    e2(3)
-    ready(0)
-    diagonal(0)
-    visits(0, 0, 1)
-    e3(1)
-    pick(0)
-    forward(1)
-    pick(1)
-    e3(2)
-    ready(1)
-    diagonal(1)
-    visits(1, 0, 5)
-    e3(3)
-    pick(2)
-    forward(2)
-    pick(3)
-    for load in loads[3:]:
-        load.wait()
-
-    @pl.loop(0, per_group)
-    def _(j):
-        value = gated(xg[j], egate[j], eup[j])
-        hidden = (value * share_buf[j]).astype(jnp.bfloat16)
-        at = pl.ds(pl.multiple_of(j * slot2, 16), slot2)
-        for part in range(4):
-            cols = slice(part * quarter, (part + 1) * quarter)
-            out = jnp.dot(
-                hidden, edown[j, :, cols], preferred_element_type=jnp.float32
-            ).astype(jnp.bfloat16)
-            for k in range(4):
-                y_buf[part % 2, part // 2, k, at, :] = out[k * slot2 : (k + 1) * slot2]
-
-    for k in (3, 2, 1, 0):
-        start(c_r1, k)
-    start(c_r1s)
+    def experts_of(chunk):
+        span = 2 * slot2
+
+        @pl.loop(0, per_group)
+        def _(j):
+            here = slice(chunk * span, (chunk + 1) * span)
+            value = gated(xg[j, here, :], egate[j], eup[j])
+            hidden = (value * share_buf[j, here, :]).astype(jnp.bfloat16)
+            at = pl.ds(pl.multiple_of(j * slot2, 16), slot2)
+            for part in range(4):
+                cols = slice(part * quarter, (part + 1) * quarter)
+                out = jnp.dot(
+                    hidden, edown[j, :, cols], preferred_element_type=jnp.float32
+                ).astype(jnp.bfloat16)
+                for k in range(2):
+                    y_buf[part % 2, part // 2, 2 * chunk + k, at, :] = out[
+                        k * slot2 : (k + 1) * slot2
+                    ]
 
     def wide(ref):
         return ref.astype(jnp.float32)
@@ -786,7 +811,11 @@
 
     def combine(k):
         c_r3(k).wait_recv()
-        u_send[k] = (term_buf[k, x] + wide(r3[k])).astype(jnp.bfloat16)
+        total = term_buf[k, x] + wide(r3[k])
+        if k == 2:
+            c_r4(3).wait_recv()
+            total = total + wide(r4[3])
+        u_send[k] = total.astype(jnp.bfloat16)
         c_r4(k).start()
 
     for k in range(4):
@@ -796,52 +825,102 @@
             started.append((c_r4, (k,)))
     started.append((c_r2s, ()))
 
+    e2(0)
+    e1(1)
+    start(kvx, 0)
+    start(qc, 1)
+    for m in range(1, 8):
+        small(m).wait_recv()
+    for k in range(4):
+        select(k)
+    e3(0)
+    e1(2)
+    start(gz, 3)
+    for k in (3, 2, 1):
+        start(kvz, k)
+        start(qc, 2 * k)
+        start(qc, 2 * k + 1)
+    e2(1)
+    ready(0)
+    pick(0)
+    e2(2)
+    diagonal(0)
+    e1(3)
+    e3(1)
+    pick(1)
+    for load in loads[3:]:
+        load.wait()
+    experts_of(0)
+    start(c_r1, 1)
+    start(c_r1, 0)
+    start(c_r1s)
+    e2(3)
     forward(3)
-    core_sum(3)
-    core_sum(2)
-    ready(2)
-    diagonal(2)
     core_sum(1)
     core_sum(0)
     shared_sum()
-    visits(2, 0, 9)
+    e3(2)
+    pick(2)
+    ready(3)
+    forward(2)
+    diagonal(3)
+    e3(3)
+    pick(3)
+    experts_of(1)
+    start(c_r1, 3)
+    start(c_r1, 2)
+    forward(1)
+    cross(3, 0)
+    core_sum(3)
+    core_sum(2)
+    scatter(1)
+    scatter(0)
+    ready(2)
+    diagonal(2)
+    cross(2, 0)
+    combine(1)
+    cross(2, 3)
     scatter(3)
-    ready(3)
-    diagonal(3)
-    visits(3, 0, 5)
+    ready(1)
+    diagonal(1)
+    scatter(2)
+    cross(1, 3)
+    epilogue(3)
+    combine(3)
+    cross(1, 2)
+    epilogue(2)
+    combine(2)
+    cross(1, 0)
+    epilogue(1)
     epilogue(0)
-    combine(3)
-    scatter(2)
-    visits(3, 5, 9)
-    epilogue(1)
-    combine(2)
-    scatter(1)
-    visits(3, 9, 13)
-    epilogue(2)
-    epilogue(3)
-    combine(1)
-    scatter(0)
     c_r2s().wait_recv()
     c_r3(0).wait_recv()
     out = term_buf[0, x] + wide(r3[0]) + wide(ysh[c, y]) + wide(r1s[y]) + wide(r2s[...])
-    for k in (3, 2, 1):
+    for k in (2, 1):
         c_r4(k).wait_recv()
         out = out + wide(r4[k])
     expert_ref[...] = out.astype(expert_ref.dtype)
 
     for m in range(1, 8):
         c_o(m).wait_recv()
+    mixed_ref[...] = o_recv[...]
+    for copy_fn, args in started:
+        copy_fn(*args).wait_send()
+
+
+def finish_kernel(parcels_ref, sum_ref, mixed_ref, expert_ref):
+    count, half, _ = parcels_ref.shape
+    low_half = lax.broadcasted_iota(jnp.int32, (half, 128), 1) < 64
     for part in range(2):
-        for head in range(0, heads, 2):
+        for head in range(0, count // 2, 2):
             lanes = slice(head // 2 * 128, head // 2 * 128 + 128)
-            first, second = o_recv[head * 2 + part], o_recv[(head + 1) * 2 + part]
-            at = part * tile
+            first, second = parcels_ref[head * 2 + part], parcels_ref[(head + 1) * 2 + part]
+            at = part * 2 * half
             mixed_ref[at : at + half, lanes] = jnp.where(low_half, first, swap_halves(second))
-            mixed_ref[at + half : at + tile, lanes] = jnp.where(
+            mixed_ref[at + half : at + 2 * half, lanes] = jnp.where(
                 low_half, swap_halves(first), second
             )
-    for copy_fn, args in started:
-        copy_fn(*args).wait_send()
+    expert_ref[...] = sum_ref[...]
 
 
 def fused(
@@ -872,30 +951,21 @@
     tile, half, quarter = rows // 2, rows // 4, model // 4
     slots = per_group * 2 * cap
     shared = shared_gate.shape[0]
-    lines = rows // 128
-    gates = cum_gate.T.reshape(heads, lines, 128)
-    named = jnp.concatenate([routes.astype(jnp.float32), route_weight], axis=1).T
-    small = jnp.concatenate(
-        [
-            jnp.broadcast_to(named, (heads, 2 * choose, 128)),
-            gates,
-            jnp.zeros((heads, 8 - lines, 128), jnp.float32),
-        ],
-        axis=1,
-    )
-    gain = head_gain.reshape(heads, 1, 64)
-    gain = jnp.concatenate([gain, gain], axis=2)
     bf16, f32 = jnp.bfloat16, jnp.float32
     vmem = pl.BlockSpec(memory_space=VMEM)
     hbm = pl.BlockSpec(memory_space=pl.ANY)
     scratch = [
+        VMEM((heads, 16, 128), f32),
         VMEM((heads, rows, 128), bf16),
         VMEM((heads, 2, half, 128), bf16),
         VMEM((devices, rows, 128), bf16),
         VMEM((devices, half, 128), bf16),
+        VMEM((devices, rows, 128), bf16),
+        VMEM((devices, 64, rows), bf16),
+        VMEM((devices, tile, 256), bf16),
         VMEM((devices, 16, 128), f32),
-        VMEM((devices, tile, 1), f32),
-        VMEM((devices, tile, 128), f32),
+        VMEM((4, 1, 2 * tile), f32),
+        VMEM((4, 64, 2 * tile), f32),
         VMEM((devices, half, 128), bf16),
         VMEM((devices, half, 128), bf16),
         VMEM((devices * tokens, model), bf16),
@@ -925,12 +995,12 @@
         pltpu.SemaphoreType.DMA((COPIES,)),
         pltpu.SemaphoreType.DMA((COPIES,)),
     ]
-    return pl.pallas_call(
+    parcels, total = pl.pallas_call(
         functools.partial(fused_kernel, cap),
-        in_specs=[vmem] * 7 + [hbm] * 6,
+        in_specs=[vmem] * 9 + [hbm] * 6,
         out_specs=(vmem, vmem),
         out_shape=(
-            jax.ShapeDtypeStruct((rows, width), bf16),
+            jax.ShapeDtypeStruct((devices, half, 128), bf16),
             jax.ShapeDtypeStruct((tokens, quarter), bf16),
         ),
         scratch_shapes=scratch,
@@ -942,8 +1012,10 @@
         queries,
         keys,
         values,
-        small,
-        gain,
+        cum_gate.T,
+        routes.T,
+        route_weight.T,
+        head_gain[None],
         moe_in,
         ffn_gain[None],
         expert_gate,
@@ -953,6 +1025,16 @@
         shared_up,
         shared_down,
     )
+    return pl.pallas_call(
+        finish_kernel,
+        in_specs=[vmem, vmem],
+        out_specs=(vmem, vmem),
+        out_shape=(
+            jax.ShapeDtypeStruct((rows, width), bf16),
+            jax.ShapeDtypeStruct((tokens, quarter), bf16),
+        ),
+        name="finish",
+    )(parcels, total)
 
 
 def fits_fused(cum_gate, queries, moe_in, routes, expert_gate):

time: 106 us -> 85 us (0.80)
  Pallas kernels: 97.3 us -> 84.2 us
  local copies, waits for them, and re-layouts: 4.89 us -> 0 us
  other arithmetic: 2.71 us -> 0 us
    pallas_call x1 -> x2, Pallas kernels: 97.3 us -> 84.2 us  [the longest x1 82.3 us: fused(): pl.pallas_call(functools.partial(fused_kernel, cap), in_specs=[vmem] * 9...]
    unnamed x2 -> x0, local copies, waits for them, and re-layouts: 3.33 us -> none
    reshape x2 -> x0, local copies, waits for them, and re-layouts: 1.47 us -> none  [the longest x1 0.76 us: fused(): gain = head_gain.reshape(heads, 1, 64)]
    concatenate x2 -> x0, other arithmetic: 1.34 us -> none  [the longest x1 0.69 us: fused(): jnp.concatenate([jnp.broadcast_to(named, (heads, 2 * choose, 128)), gates...]
where the time goes in v2:
time: 85 us; the launch traced here: 84.9 us
  Pallas kernels  84.2 us (99%)
    pallas_call x1, Pallas kernels, fused(): pl.pallas_call(functools.partial(fused_kernel, cap), in_specs=[vmem] * 9...  82.3 us
    pallas_call x1, Pallas kernels, fused(): pl.pallas_call(finish_kernel, in_specs=[vmem, vmem], out_specs=(vmem, vme...  1.94 us

profile of v2, /device:TPU:0, one launch (start us, length us, event | category | flops | bytes accessed | tf_op | source)
XLA Modules:
  0.0 84.9 jit_solution(9642544208887641753)
XLA Ops:
  0.6 82.3 %fused.1 = (bf16[8,192,128]{2,1,0:T(8,128)(2,1)}, bf16[128,512]{1,0:T(8,128)(2,1)}) custom-call(bf16[768,256]{1,0:T(8,128)(2,1)} %q_ref.1, bf16[768,256]{1,0:T(8,128)(2,1)} %k_ref.1, bf16[768,256]{1,0:T(8,128)(2,1)} %v_ref.1, f32[4,768]{1,0:T(4,128)} %bitcast.5, s32[4,128]{1,0:T(4,128)} %bitcast.7, f32[4,128]{1,0:T(4,128)} %bitcast.8, f32[1,256]{1,0:T(1,128)} %bitcast.9, ...), custom_call_target="tpu_custom_call" | custom-call | tf_op jit(solution)/shard_map/fused/pallas_call | solution.py:998
  82.9 1.9 %finish.1 = (bf16[768,256]{1,0:T(8,128)(2,1)}, bf16[128,512]{1,0:T(8,128)(2,1)}) custom-call(bf16[8,192,128]{2,1,0:T(8,128)(2,1)} %get-tuple-element.4.parcels_ref, bf16[128,512]{1,0:T(8,128)(2,1)} %get-tuple-element.5.sum_ref), custom_call_target="tpu_custom_call" | custom-call | tf_op jit(solution)/shard_map/finish/pallas_call | solution.py:1028

commit v3 on v2

--- a/solution.py
+++ b/solution.py
@@ -340,15 +340,15 @@
 
 def fused_kernel(
     cap,
-    q_ref,
-    k_ref,
-    v_ref,
-    cum_ref,
-    routes_ref,
-    weight_ref,
-    gain_ref,
-    moe_ref,
-    ffn_ref,
+    moe_hbm,
+    ffn_hbm,
+    routes_hbm,
+    weight_hbm,
+    cum_hbm,
+    k_hbm,
+    v_hbm,
+    q_hbm,
+    gain_hbm,
     egate_hbm,
     eup_hbm,
     edown_hbm,
@@ -357,6 +357,15 @@
     sdown_hbm,
     mixed_ref,
     expert_ref,
+    moe_ref,
+    ffn_ref,
+    routes_ref,
+    weight_ref,
+    cum_ref,
+    k_ref,
+    v_ref,
+    q_ref,
+    gain_ref,
     small_ref,
     kvs,
     qs,
@@ -510,27 +519,38 @@
     for other in (ty, tc):
         pl.semaphore_signal(barrier, inc=1, device_id={"tp": other}, device_id_type=MESH)
 
+    inputs = (
+        (moe_hbm, moe_ref),
+        (ffn_hbm, ffn_ref),
+        (routes_hbm, routes_ref),
+        (weight_hbm, weight_ref),
+        (cum_hbm, cum_ref),
+        (k_hbm, k_ref),
+        (v_hbm, v_ref),
+        (q_hbm, q_ref),
+        (gain_hbm, gain_ref),
+        (sgate_hbm, sgate),
+        (sup_hbm, sup),
+        (sdown_hbm, sdown),
+        (egate_hbm, egate),
+        (eup_hbm, eup),
+        (edown_hbm, edown),
+    )
     loads = [
-        pltpu.make_async_copy(src, dst, wsem.at[n])
-        for n, (src, dst) in enumerate(
-            (
-                (sgate_hbm, sgate),
-                (sup_hbm, sup),
-                (sdown_hbm, sdown),
-                (egate_hbm, egate),
-                (eup_hbm, eup),
-                (edown_hbm, edown),
-            )
-        )
+        pltpu.make_async_copy(src, dst, wsem.at[n]) for n, (src, dst) in enumerate(inputs)
     ]
     for load in loads:
         load.start()
 
+    for load in loads[:2]:
+        load.wait()
     own = moe_ref[...].astype(jnp.float32)
     square = jnp.sum(own * own, axis=1, keepdims=True) / model
     own = (own * lax.rsqrt(square + NORM_EPSILON) * ffn_ref[...]).astype(jnp.bfloat16)
     own_rows = pl.ds(pl.multiple_of(e * tokens, tokens), tokens)
     x_all[own_rows, :] = own
+    for load in loads[2:5]:
+        load.wait()
 
     lines = rows // 128
     for head in range(heads):
@@ -543,6 +563,15 @@
         )
     small_all[e] = small_ref[z]
 
+    pl.semaphore_wait(barrier, 9)
+    for m in (7, 6, 5, 4, 3, 2, 1):
+        start(small, m)
+    start(gz, 1)
+    start(gz, 2)
+    start(gx, 0)
+
+    for load in loads[5:9]:
+        load.wait()
     low = lax.broadcasted_iota(jnp.int32, (rows, 128), 1) < 64
     low_half = low[:half]
     for head in range(heads):
@@ -563,13 +592,6 @@
             qs[head, part] = packed
     kv_all[e] = kvs[z]
     q_all[e] = qs[z, x]
-    pl.semaphore_wait(barrier, 9)
-    for m in (7, 6, 5, 4, 3, 2, 1):
-        start(small, m)
-    start(gz, 1)
-    start(gz, 2)
-    start(gx, 0)
-
     lane = lax.broadcasted_iota(jnp.int32, (1, 128), 1)
     spread = jnp.where(
         lax.broadcasted_iota(jnp.int32, (16, 128), 0) + 64
@@ -755,7 +777,7 @@
             prep_kv(peer(m))
             prep_q(peer(m))
 
-    for load in loads[:3]:
+    for load in loads[9:12]:
         load.wait()
     shared_hidden = gated(x_all[own_rows, :], sgate[...], sup[...]).astype(jnp.bfloat16)
     for part in range(4):
@@ -766,7 +788,7 @@
     def experts_of(chunk):
         span = 2 * slot2
 
-        @pl.loop(0, per_group)
+        @pl.loop(0, per_group, unroll=2)
         def _(j):
             here = slice(chunk * span, (chunk + 1) * span)
             value = gated(xg[j, here, :], egate[j], eup[j])
@@ -825,71 +847,71 @@
             started.append((c_r4, (k,)))
     started.append((c_r2s, ()))
 
-    e2(0)
-    e1(1)
-    start(kvx, 0)
-    start(qc, 1)
+    start(c_r1s)
     for m in range(1, 8):
         small(m).wait_recv()
     for k in range(4):
         select(k)
-    e3(0)
+    shared_sum()
+    e2(0)
     e1(2)
     start(gz, 3)
+    e1(1)
     for k in (3, 2, 1):
         start(kvz, k)
         start(qc, 2 * k)
-        start(qc, 2 * k + 1)
+    e3(0)
+    e2(2)
+    pick(0)
+    e1(3)
+    start(kvx, 0)
+    for m in (1, 7, 5, 3):
+        start(qc, m)
+    e2(3)
     e2(1)
+    e3(2)
+    pick(2)
     ready(0)
-    pick(0)
-    e2(2)
     diagonal(0)
-    e1(3)
+    forward(3)
+    e3(3)
+    for load in loads[12:]:
+        load.wait()
+    pick(3)
+    experts_of(1)
     e3(1)
+    start(c_r1, 3)
+    start(c_r1, 2)
+    ready(3)
+    diagonal(3)
+    core_sum(3)
+    core_sum(2)
     pick(1)
-    for load in loads[3:]:
-        load.wait()
+    forward(2)
     experts_of(0)
     start(c_r1, 1)
     start(c_r1, 0)
-    start(c_r1s)
-    e2(3)
-    forward(3)
+    forward(1)
+    ready(2)
+    scatter(3)
     core_sum(1)
     core_sum(0)
-    shared_sum()
-    e3(2)
-    pick(2)
-    ready(3)
-    forward(2)
-    diagonal(3)
-    e3(3)
-    pick(3)
-    experts_of(1)
-    start(c_r1, 3)
-    start(c_r1, 2)
-    forward(1)
+    diagonal(2)
     cross(3, 0)
-    core_sum(3)
-    core_sum(2)
+    scatter(2)
+    cross(2, 0)
+    combine(3)
+    cross(2, 3)
     scatter(1)
-    scatter(0)
-    ready(2)
-    diagonal(2)
-    cross(2, 0)
-    combine(1)
-    cross(2, 3)
-    scatter(3)
     ready(1)
     diagonal(1)
-    scatter(2)
+    combine(2)
+    scatter(0)
     cross(1, 3)
     epilogue(3)
-    combine(3)
+    combine(1)
     cross(1, 2)
     epilogue(2)
-    combine(2)
     cross(1, 0)
     epilogue(1)
     epilogue(0)
@@ -955,6 +977,15 @@
     vmem = pl.BlockSpec(memory_space=VMEM)
     hbm = pl.BlockSpec(memory_space=pl.ANY)
     scratch = [
+        VMEM((tokens, model), bf16),
+        VMEM((1, model), f32),
+        VMEM((choose, tokens), jnp.int32),
+        VMEM((choose, tokens), f32),
+        VMEM((heads, rows), f32),
+        VMEM((rows, width), bf16),
+        VMEM((rows, width), bf16),
+        VMEM((rows, width), bf16),
+        VMEM((1, width), f32),
         VMEM((heads, 16, 128), f32),
         VMEM((heads, rows, 128), bf16),
         VMEM((heads, 2, half, 128), bf16),
@@ -991,13 +1022,13 @@
         VMEM((4, tokens, quarter), bf16),
         VMEM((4, tokens, quarter), bf16),
         VMEM((4, tokens, quarter), bf16),
-        pltpu.SemaphoreType.DMA((6,)),
+        pltpu.SemaphoreType.DMA((15,)),
         pltpu.SemaphoreType.DMA((COPIES,)),
         pltpu.SemaphoreType.DMA((COPIES,)),
     ]
     parcels, total = pl.pallas_call(
         functools.partial(fused_kernel, cap),
-        in_specs=[vmem] * 9 + [hbm] * 6,
+        in_specs=[hbm] * 15,
         out_specs=(vmem, vmem),
         out_shape=(
             jax.ShapeDtypeStruct((devices, half, 128), bf16),
@@ -1009,15 +1040,15 @@
         ),
         name="fused",
     )(
-        queries,
+        moe_in,
+        ffn_gain[None],
+        routes.T,
+        route_weight.T,
+        cum_gate.T,
         keys,
         values,
-        cum_gate.T,
-        routes.T,
-        route_weight.T,
+        queries,
         head_gain[None],
-        moe_in,
-        ffn_gain[None],
         expert_gate,
         expert_up,
         expert_down,

time: 85 us -> 80.9 us (0.952)
  Pallas kernels: 84.2 us -> 80.1 us
    pallas_call x1, Pallas kernels: 82.3 us -> 78.2 us  [fused(): pl.pallas_call(functools.partial(fused_kernel, cap), in_specs=[hbm] * 15,...]
where the time goes in v3:
time: 80.9 us; the launch traced here: 80.8 us
  Pallas kernels  80.1 us (99%)
    pallas_call x1, Pallas kernels, fused(): pl.pallas_call(functools.partial(fused_kernel, cap), in_specs=[hbm] * 15,...  78.2 us
    pallas_call x1, Pallas kernels, fused(): pl.pallas_call(finish_kernel, in_specs=[vmem, vmem], out_specs=(vmem, vme...  1.94 us

profile of v3, /device:TPU:0, one launch (start us, length us, event | category | flops | bytes accessed | tf_op | source)
XLA Modules:
  0.0 80.8 jit_solution(11067906622195867768)
XLA Ops:
  0.6 78.2 %fused.1 = (bf16[8,192,128]{2,1,0:T(8,128)(2,1)}, bf16[128,512]{1,0:T(8,128)(2,1)}) custom-call(bf16[128,2048]{1,0:T(8,128)(2,1)} %moe_hbm.1, f32[1,2048]{1,0:T(1,128)} %bitcast.6, s32[4,128]{1,0:T(4,128)} %bitcast.7, f32[4,128]{1,0:T(4,128)} %bitcast.8, f32[4,768]{1,0:T(4,128)} %bitcast.5, bf16[768,256]{1,0:T(8,128)(2,1)} %k_hbm.1, bf16[768,256]{1,0:T(8,128)(2,1)} %v_hbm.1, ...), custom_call_target="tpu_custom_call" | custom-call | tf_op jit(solution)/shard_map/fused/pallas_call | solution.py:1029
  78.8 1.9 %finish.1 = (bf16[768,256]{1,0:T(8,128)(2,1)}, bf16[128,512]{1,0:T(8,128)(2,1)}) custom-call(bf16[8,192,128]{2,1,0:T(8,128)(2,1)} %get-tuple-element.4.parcels_ref, bf16[128,512]{1,0:T(8,128)(2,1)} %get-tuple-element.5.sum_ref), custom_call_target="tpu_custom_call" | custom-call | tf_op jit(solution)/shard_map/finish/pallas_call | solution.py:1059

commit v4 on v3

--- a/solution.py
+++ b/solution.py
@@ -899,13 +899,13 @@
     diagonal(2)
     cross(3, 0)
     scatter(2)
+    combine(3)
     cross(2, 0)
-    combine(3)
     cross(2, 3)
     scatter(1)
+    combine(2)
     ready(1)
     diagonal(1)
-    combine(2)
     scatter(0)
     cross(1, 3)
     epilogue(3)

time: 80.9 us -> 80.9 us (level)
  no operation moved by 1% of the time
where the time goes in v4:
time: 80.9 us; the launch traced here: 80.8 us
  Pallas kernels  80.1 us (99%)
    pallas_call x1, Pallas kernels, fused(): pl.pallas_call(functools.partial(fused_kernel, cap), in_specs=[hbm] * 15,...  78.2 us
    pallas_call x1, Pallas kernels, fused(): pl.pallas_call(finish_kernel, in_specs=[vmem, vmem], out_specs=(vmem, vme...  1.94 us

profile of v4, /device:TPU:0, one launch (start us, length us, event | category | flops | bytes accessed | tf_op | source)
XLA Modules:
  0.0 80.8 jit_solution(4718513111170161172)
XLA Ops:
  0.6 78.2 %fused.1 = (bf16[8,192,128]{2,1,0:T(8,128)(2,1)}, bf16[128,512]{1,0:T(8,128)(2,1)}) custom-call(bf16[128,2048]{1,0:T(8,128)(2,1)} %moe_hbm.1, f32[1,2048]{1,0:T(1,128)} %bitcast.6, s32[4,128]{1,0:T(4,128)} %bitcast.7, f32[4,128]{1,0:T(4,128)} %bitcast.8, f32[4,768]{1,0:T(4,128)} %bitcast.5, bf16[768,256]{1,0:T(8,128)(2,1)} %k_hbm.1, bf16[768,256]{1,0:T(8,128)(2,1)} %v_hbm.1, ...), custom_call_target="tpu_custom_call" | custom-call | tf_op jit(solution)/shard_map/fused/pallas_call | solution.py:1029
  78.8 1.9 %finish.1 = (bf16[768,256]{1,0:T(8,128)(2,1)}, bf16[128,512]{1,0:T(8,128)(2,1)}) custom-call(bf16[8,192,128]{2,1,0:T(8,128)(2,1)} %get-tuple-element.4.parcels_ref, bf16[128,512]{1,0:T(8,128)(2,1)} %get-tuple-element.5.sum_ref), custom_call_target="tpu_custom_call" | custom-call | tf_op jit(solution)/shard_map/finish/pallas_call | solution.py:1059
